TPU v7x, 32 devices: a whole 2x2x4 slice. The times are simulated.
32 devices in a mesh: ep: 8 (over z, x), tp: 4 (over y, core).
Axes of the slice: x: 2, y: 2, z: 4, core: 2. Of those that a mesh axis runs over, the one named last changes fastest.
Arguments:
- queries: bfloat16 [2048, 1024], P('ep', 'tp'), may hold values from -6 to 6
- keys: bfloat16 [2048, 256], P('ep', 'tp'), may hold values from -6 to 6
- values: bfloat16 [2048, 256], P('ep', 'tp'), may hold values from -6 to 6
- q_gain: float32 [64], replicated, may hold values from 1 to 6
- k_gain: float32 [64], replicated, may hold values from 1 to 6
- out_weight: bfloat16 [1024, 2048], P('tp'), may hold values from -0.1875 to 0.1875
- tokens: bfloat16 [1024, 2048], P(('ep', 'tp')), may hold values from -6 to 6
- ffn_gain: float32 [2048], replicated, may hold values from 0.1 to 1.9
- route: int32 [1024, 2], P(('ep', 'tp')), may hold values from 0 to 7, all different within a row; in each aligned block of 32 rows (0 to 31, 32 to 63, ...) at most 16 rows name the same one
- route_weight: float32 [1024, 2], P(('ep', 'tp')), may hold values from 0.1 to 1
- gate_weight: bfloat16 [8, 2048, 3584], P('ep', None, 'tp'), may hold values from -0.125 to 0.125
- up_weight: bfloat16 [8, 2048, 3584], P('ep', None, 'tp'), may hold values from -0.125 to 0.125
- down_weight: bfloat16 [8, 3584, 2048], P('ep', 'tp'), may hold values from -0.09375 to 0.09375
Outputs:
- mixer_out: bfloat16 [2048, 2048], P(('ep', 'tp'))
- mixed: bfloat16 [1024, 2048], P(('ep', 'tp'))
Inputs may be any that keep to these rules, and one draw needn't show every extreme that they name: `route`: each row names 2 different experts. In every device's aligned block of 32 rows no expert is named more than 16 times, and in some blocks some expert is named exactly 16 times.
All inputs are finite; a program needn't handle non-finite values.
Results may differ from a plain program's by a relative error of at most 0.013.
The roundings to bfloat16 on the way count: a program that leaves them out, or rounds other values in their place, can miss the bound.
Values may be sent and summed in bfloat16 or wider, within the bound.
No kernel may reach another device: no remote copies, remote signals or barrier semaphores. Data moves between devices by JAX's collectives and lax.ppermute only.
A program may use at most 192 MiB of HBM per device.

v0:
```python
import jax
import jax.numpy as jnp
from jax import lax
from jax.sharding import PartitionSpec as P

GRID_W = 64
EPS = 1e-06
THETA = 10000.0


def head_norm(vals, gain):
    vals = vals.astype(jnp.float32)
    return vals * lax.rsqrt(jnp.mean(vals * vals, axis=-1, keepdims=True) + EPS) * gain


def rotate(vals, positions):
    pairs = vals.shape[-1] // 2
    quarter = pairs // 2
    freqs = THETA ** (-jnp.arange(quarter, dtype=jnp.float32) / quarter)
    grid_row = (positions // GRID_W).astype(jnp.float32)
    grid_col = (positions % GRID_W).astype(jnp.float32)
    angle = jnp.concatenate([grid_row[:, None] * freqs, grid_col[:, None] * freqs], axis=-1)
    cosine = jnp.cos(angle)[:, None, :]
    sine = jnp.sin(angle)[:, None, :]
    split = vals.reshape(vals.shape[:-1] + (pairs, 2))
    first = split[..., 0]
    second = split[..., 1]
    turned = jnp.stack([first * cosine - second * sine, first * sine + second * cosine], axis=-1)
    return turned.reshape(vals.shape)


def local(
    queries,
    keys,
    values,
    q_gain,
    k_gain,
    out_weight,
    tokens,
    ffn_gain,
    route,
    route_weight,
    gate_weight,
    up_weight,
    down_weight,
):
    local_rows = queries.shape[0]
    head_size = q_gain.shape[0]
    query_heads = queries.shape[1] // head_size
    key_heads = keys.shape[1] // head_size
    group = query_heads // key_heads
    key_width = key_heads * head_size
    positions = lax.axis_index("ep") * local_rows + jnp.arange(local_rows, dtype=jnp.int32)
    rot_q = rotate(
        head_norm(queries.reshape(local_rows, query_heads, head_size), q_gain), positions
    ).astype(jnp.bfloat16)
    rot_q = rot_q.reshape(local_rows, key_heads, group, head_size)
    rot_k = rotate(
        head_norm(keys.reshape(local_rows, key_heads, head_size), k_gain), positions
    ).astype(jnp.bfloat16)
    joined = jnp.concatenate([rot_k.reshape(local_rows, key_width), values], axis=1)
    scale = head_size ** (-0.5)

    def fold_block(carry, block):
        highest, denom, numer = carry
        key_block = block[:, :key_width].reshape(-1, key_heads, head_size)
        value_block = block[:, key_width:].reshape(-1, key_heads, head_size)
        scores = (
            jnp.einsum("qkgd,skd->qkgs", rot_q, key_block, preferred_element_type=jnp.float32)
            * scale
        )
        new_high = jnp.maximum(highest, jnp.max(scores, axis=-1))
        shrink = jnp.exp(highest - new_high)
        expo = jnp.exp(scores - new_high[..., None])
        denom = denom * shrink + jnp.sum(expo, axis=-1)
        numer = numer * shrink[..., None] + jnp.einsum(
            "qkgs,skd->qkgd",
            expo.astype(jnp.bfloat16),
            value_block,
            preferred_element_type=jnp.float32,
        )
        return ((new_high, denom, numer), None)

    start_high = jnp.full((local_rows, key_heads, group), -1e30, jnp.float32)
    start_denom = jnp.zeros((local_rows, key_heads, group), jnp.float32)
    start_numer = jnp.zeros((local_rows, key_heads, group, head_size), jnp.float32)
    carry = (start_high, start_denom, start_numer)
    piece = lax.all_gather(joined, "ep", axis=0, tiled=True)
    length = piece.shape[0]
    size = length
    while size > 2048 and size % 2 == 0:
        size = size // 2
    blocks = piece.reshape(length // size, size, piece.shape[1])
    carry, _ = lax.scan(fold_block, carry, blocks)
    highest, denom, numer = carry
    attended = (
        (numer / denom[..., None]).astype(jnp.bfloat16).reshape(local_rows, query_heads * head_size)
    )
    own_rows = tokens.shape[0]
    width = tokens.shape[1]
    picks_row = route.shape[1]
    experts = lax.axis_size("ep")
    capacity = 2 * own_rows * picks_row // experts
    token_float = tokens.astype(jnp.float32)
    normed = (
        token_float
        * lax.rsqrt(jnp.mean(token_float * token_float, axis=-1, keepdims=True) + EPS)
        * ffn_gain
    ).astype(jnp.bfloat16)
    flat_route = route.reshape(-1)
    expert_hot = (flat_route[:, None] == jnp.arange(experts, dtype=jnp.int32)[None, :]).astype(
        jnp.int32
    )
    earlier = jnp.cumsum(expert_hot, axis=0) - expert_hot
    rank = jnp.sum(earlier * expert_hot, axis=1)
    slot = flat_route * capacity + rank
    pick_hot = (slot[:, None] == jnp.arange(experts * capacity, dtype=jnp.int32)[None, :]).astype(
        jnp.bfloat16
    )
    row_hot = jnp.sum(pick_hot.reshape(own_rows, picks_row, experts * capacity), axis=1)
    outgoing = jnp.einsum("rs,rd->sd", row_hot, normed, preferred_element_type=jnp.float32).astype(
        jnp.bfloat16
    )
    outgoing = outgoing.reshape(experts, capacity, width)
    gate_local = gate_weight[0]
    up_local = up_weight[0]
    down_local = down_weight[0]
    arrived = lax.all_to_all(outgoing, "ep", split_axis=0, concat_axis=0, tiled=True)
    sources = arrived.shape[0]
    items = arrived.shape[1]
    slot_rows = arrived.reshape(sources * items, width)
    piece = lax.all_gather(slot_rows, "tp", axis=0, tiled=True)
    gate = jnp.dot(piece, gate_local, preferred_element_type=jnp.float32)
    upper = jnp.dot(piece, up_local, preferred_element_type=jnp.float32)
    hidden = (jax.nn.silu(gate) * upper).astype(jnp.bfloat16)
    worked = jnp.dot(hidden, down_local, preferred_element_type=jnp.float32).reshape(
        -1, items, width
    )
    head_partial = jnp.dot(attended, out_weight, preferred_element_type=jnp.float32)
    mixer_sum, expert_sum = (
        lax.psum_scatter(
            head_partial.astype(jnp.bfloat16), "tp", scatter_dimension=0, tiled=True
        ).astype(jnp.float32),
        lax.psum_scatter(worked.astype(jnp.bfloat16), "tp", scatter_dimension=0, tiled=True).astype(
            jnp.float32
        ),
    )
    mixer_out = mixer_sum.astype(jnp.bfloat16)
    home = expert_sum.astype(jnp.bfloat16)
    back = lax.all_to_all(home, "ep", split_axis=0, concat_axis=0, tiled=True)
    copies = jnp.dot(
        pick_hot, back.reshape(experts * capacity, width), preferred_element_type=jnp.float32
    )
    weighted = route_weight[..., None] * copies.reshape(own_rows, picks_row, width)
    mixed = jnp.sum(weighted, axis=1).astype(jnp.bfloat16)
    return (mixer_out, mixed)


def solution(mesh):
    placed = (
        P("ep", "tp"),
        P("ep", "tp"),
        P("ep", "tp"),
        P(),
        P(),
        P("tp", None),
        P(("ep", "tp"), None),
        P(),
        P(("ep", "tp"), None),
        P(("ep", "tp"), None),
        P("ep", None, "tp"),
        P("ep", None, "tp"),
        P("ep", "tp", None),
    )
    return jax.shard_map(
        local,
        mesh=mesh,
        in_specs=placed,
        out_specs=(P(("ep", "tp"), None), P(("ep", "tp"), None)),
        check_vma=False,
    )
```

profile of v0, /device:TPU:0, one launch (start us, length us, event | category | flops | bytes accessed | tf_op | source)
XLA Modules:
  0.0 136.9 jit_solution(23721503916896512)
XLA Ops:
  7.2 0.8 copy.46
  8.3 0.2 select_reduce_fusion
  8.7 0.7 multiply_add_fusion
  9.5 1.0 fusion.30
  10.5 1.3 convolution_convert_fusion.1
  11.8 21.7 %all_to_all.10 = bf16[8,16,2048]{2,1,0:T(8,128)(2,1)} all-to-all(bf16[8,16,2048]{2,1,0:T(8,128)(2,1)S(1)} %bitcast.99), channel_id=1, replica_groups=mesh['ep'=8,'tp'=4] {'ep'}, dimensions={0} | all-to-all | bytes 1048576 | tf_op jit(solution)/shard_map/all_to_all | solution.py:128
  33.6 1.0 copy.44
  34.7 0.8 mul.273
  35.6 0.2 multiply_multiply_fusion
  35.8 19.5 %all-gather.2.cloned.1.call-done = bf16[512,2048]{1,0:T(8,128)(2,1)} async-done(((bf16[128,2048]{1,0:T(8,128)(2,1)}), bf16[512,2048]{1,0:T(8,128)(2,1)}) %all-gather.2.cloned.1.call-update) | async-done | bytes 2097168 | tf_op jit(solution)/shard_map/all_gather | solution.py:132
  55.3 5.1 %fusion.10 = f32[512,896]{1,0:T(8,128)S(1)} fusion(bf16[512,2048]{1,0:T(8,128)(2,1)} %all-gather.2.cloned.1.call-done, bf16[1,2048,896]{2,1,0:T(8,128)(2,1)} %param.23), kind=kOutput, calls=%fused_computation.11 | convolution fusion | flops 1879048192 | bytes 7602176 | tf_op jit(solution)/shard_map/dot_general | solution.py:133
  60.5 2.4 %multiply_convert_fusion = bf16[512,896]{1,0:T(8,128)(2,1)S(1)} fusion(f32[512,896]{1,0:T(8,128)S(1)} %fusion.10, bf16[512,2048]{1,0:T(8,128)(2,1)S(1)} %copy-done.7, bf16[1,2048,896]{2,1,0:T(8,128)(2,1)S(1)} %copy-done.5), kind=kOutput, calls=%fused_computation.17 | convolution fusion | flops 1881800704 | bytes 8519680 | tf_op jit(solution)/shard_map/dot_general | solution.py:134
  62.9 3.7 %fusion.12 = bf16[32,16,2048]{2,1,0:T(8,128)(2,1)} fusion(bf16[32,16,896]{2,1,0:T(8,128)(2,1)S(1)} %bitcast.101, bf16[1,896,2048]{2,1,0:T(8,128)(2,1)S(1)} %copy-done.6), kind=kOutput, calls=%fused_computation.13 | convolution fusion | flops 1880096768 | bytes 6684672 | tf_op jit(solution)/shard_map/dot_general | solution.py:136
  66.9 0.3 subtract_convert_fusion
  67.3 0.3 pad_maximum_fusion
  67.8 0.1 subtract_convert_fusion.1
  68.1 31.6 %all_gather.6 = bf16[2048,128]{0,1:T(8,128)(2,1)S(1)} all-gather(bf16[256,128]{0,1:T(8,128)(2,1)S(1)} %pad_maximum_fusion.1), channel_id=1, replica_groups=mesh['ep'=8,'tp'=4] {'ep'}, dimensions={0}, use_global_device_ids=true | all-gather | bytes 589824 | tf_op jit(solution)/shard_map/all_gather | solution.py:88
  99.7 1.3 bitcast_reduce_fusion
  101.0 1.4 %fusion.1 = f32[256,4]{0,1:T(4,128)S(1)} fusion(f32[2048,256,4]{1,0,2:T(8,128)S(1)} %get-tuple-element.37, f32[256,4]{0,1:T(4,128)S(1)} %broadcast_maximum_fusion), kind=kLoop, calls=%fused_computation.3 | loop fusion | flops 6290432 | bytes 8396800 | tf_op jit(solution)/shard_map/while/body/eval_jaxpr/reduce_sum | solution.py:75
  102.4 1.5 %fusion.27 = bf16[1,64,256,4]{2,1,3,0:T(8,128)(2,1)S(1)} fusion(f32[2048,256,4]{1,0,2:T(8,128)S(1)} %get-tuple-element.37, f32[256,4]{0,1:T(4,128)S(1)} %broadcast_maximum_fusion, bf16[2048,128]{0,1:T(8,128)(2,1)S(1)} %all_gather.6, f32[256,4]{0,1:T(4,128)S(1)} %get-tuple-element.29, f32[256,4]{0,1:T(4,128)S(1)} %get-tuple-element.28), kind=kOutput, calls=%fused_computation.22 | convolution fusion | flops 274923520 | bytes 8794112 | tf_op jit(solution)/shard_map/while/body/eval_jaxpr/qkgs,skd->qkgd/dot_general | solution.py:76
  104.0 1.4 %convolution_convert_fusion = bf16[256,2048]{1,0:T(8,128)(2,1)} fusion(bf16[256,256]{0,1:T(8,128)(2,1)S(1)} %bitcast.100, bf16[256,2048]{1,0:T(8,128)(2,1)S(1)} %copy-done), kind=kOutput, calls=%fused_computation.14 | convolution fusion | flops 268959744 | bytes 2228224 | tf_op jit(solution)/shard_map/dot_general | solution.py:139
  105.5 15.8 %all_to_all.11 = bf16[8,16,2048]{2,1,0:T(8,128)(2,1)S(1)} all-to-all(bf16[8,16,2048]{2,1,0:T(8,128)(2,1)} %reduce-scatter.5.cloned.1.call-done), channel_id=1, replica_groups=mesh['ep'=8,'tp'=4] {'ep'}, dimensions={0} | all-to-all | bytes 1048576 | tf_op jit(solution)/shard_map/all_to_all | solution.py:150
  121.3 0.9 fusion.17
  122.2 8.1 %reduce-scatter.3.cloned.1.call-done = bf16[64,2048]{1,0:T(8,128)(2,1)} async-done(((bf16[256,2048]{1,0:T(8,128)(2,1)}), bf16[64,2048]{1,0:T(8,128)(2,1)}) %reduce-scatter.3.cloned.1.call-update) | async-done | bytes 262160 | tf_op jit(solution)/shard_map/reduce_scatter | solution.py:141
  (49 shorter events, 1.5 us)
Async XLA Ops:
  7.2 96.8 %copy-start = (bf16[256,2048]{1,0:T(8,128)(2,1)S(1)}, bf16[256,2048]{1,0:T(8,128)(2,1)}, u32[]{:S(2)}) copy-start(bf16[256,2048]{1,0:T(8,128)(2,1)} %param.18) | copy-start | bytes 3145732
  7.2 48.1 %all-gather.2.cloned.1.call-start = ((), (), s32[]{:S(2)}) async-start(), calls=%async_computation.5 | async-start | bytes 2621440 | tf_op jit(solution)/shard_map/all_gather | solution.py:132
  33.5 71.9 %reduce-scatter.5.cloned.1.call-start = ((), (), s32[]{:S(2)}) async-start(), calls=%async_computation.6 | async-start | bytes 2621440 | tf_op jit(solution)/shard_map/reduce_scatter | solution.py:144
  55.3 5.2 %copy-start.5 = (bf16[1,2048,896]{2,1,0:T(8,128)(2,1)S(1)}, bf16[1,2048,896]{2,1,0:T(8,128)(2,1)}, u32[]{:S(2)}) copy-start(bf16[1,2048,896]{2,1,0:T(8,128)(2,1)} %param.24) | copy-start | bytes 11010052
  55.3 5.2 %copy-start.7 = (bf16[512,2048]{1,0:T(8,128)(2,1)S(1)}, bf16[512,2048]{1,0:T(8,128)(2,1)}, u32[]{:S(2)}) copy-start(bf16[512,2048]{1,0:T(8,128)(2,1)} %all-gather.2.cloned.1.call-done) | copy-start | bytes 6291460
  60.5 2.4 %copy-start.6 = (bf16[1,896,2048]{2,1,0:T(8,128)(2,1)S(1)}, bf16[1,896,2048]{2,1,0:T(8,128)(2,1)}, u32[]{:S(2)}) copy-start(bf16[1,896,2048]{2,1,0:T(8,128)(2,1)} %param.25) | copy-start | bytes 11010052
  62.9 4.7 %copy-start.1 = (bf16[256,64]{0,1:T(8,128)(2,1)S(1)}, bf16[256,64]{0,1:T(8,128)(2,1)}, u32[]{:S(2)}) copy-start(bf16[256,64]{0,1:T(8,128)(2,1)} %param.14) | copy-start | bytes 98308
  62.9 4.7 %copy-start.4 = (f32[64]{0:T(128)S(1)}, f32[64]{0:T(128)}, u32[]{:S(2)}) copy-start(f32[64]{0:T(128)} %param.17) | copy-start | bytes 772
  66.6 1.5 %copy-start.2 = (bf16[256,64]{0,1:T(8,128)(2,1)S(1)}, bf16[256,64]{0,1:T(8,128)(2,1)}, u32[]{:S(2)}) copy-start(bf16[256,64]{0,1:T(8,128)(2,1)} %param.15) | copy-start | bytes 98308
  66.6 63.7 %reduce-scatter.3.cloned.1.call-start = ((), (), s32[]{:S(2)}) async-start(), calls=%async_computation.4 | async-start | bytes 1310720 | tf_op jit(solution)/shard_map/reduce_scatter | solution.py:141
  103.9 17.3 %copy-start.3 = (f32[32,2]{0,1:T(2,128)S(1)}, f32[32,2]{0,1:T(2,128)}, u32[]{:S(2)}) copy-start(f32[32,2]{0,1:T(2,128)} %param.22) | copy-start | bytes 772
Sparse Core Ops, SparseCore 0:
  33.7 21.5 all-gather.1
  66.8 31.1 reduce-scatter.4
  105.6 24.7 reduce-scatter.2
where the time goes:
time: 137 us
  blocking collectives  69.1 us (50%)
  waiting for transfers between devices  27.7 us (20%)
  matrix products  17.7 us (13%)
  between operations  14 us (10%)
  other arithmetic  4.93 us (4%)
  local copies, waits for them, and re-layouts  3.26 us (2%)
    all_gather x1, blocking collectives, local(): piece = lax.all_gather(joined, 'ep', axis=0, tiled=True)  31.6 us
    all_to_all x1, blocking collectives, local(): lax.all_to_all(outgoing, 'ep', split_axis=0, concat_axis=0, tiled=True)  21.7 us
    all_gather x1, waiting for transfers between devices, local(): piece = lax.all_gather(slot_rows, 'tp', axis=0, tiled=True)  19.5 us
    all_to_all x1, blocking collectives, local(): back = lax.all_to_all(home, 'ep', split_axis=0, concat_axis=0, tiled=True)  15.8 us
    reduce_scatter x1, waiting for transfers between devices, local(): lax.psum_scatter(head_partial.astype(jnp.bfloat16), 'tp', scatter_dimensi...  8.13 us
    dot_general x1, matrix products, local(): gate = jnp.dot(piece, gate_local, preferred_element_type=jnp.float32)  5.14 us
    dot_general x1, matrix products, local(): jnp.dot(hidden, down_local, preferred_element_type=jnp.float32)  3.69 us
  transfers between devices with their start and end apart: 3, of which 2 were waited for; matrix products, arithmetic and copies ran while one was open for 7% of the time, Pallas kernels for 0%

commit v1 on v0

--- a/solution.py
+++ b/solution.py
@@ -6,6 +6,11 @@
 GRID_W = 64
 EPS = 1e-06
 THETA = 10000.0
+
+
+def gather_by_exchange(x, axis, dim):
+    copies = jnp.concatenate([x] * lax.axis_size(axis), axis=dim)
+    return lax.all_to_all(copies, axis, dim, dim, tiled=True)
 
 
 def head_norm(vals, gain):
@@ -85,7 +90,7 @@
     start_denom = jnp.zeros((local_rows, key_heads, group), jnp.float32)
     start_numer = jnp.zeros((local_rows, key_heads, group, head_size), jnp.float32)
     carry = (start_high, start_denom, start_numer)
-    piece = lax.all_gather(joined, "ep", axis=0, tiled=True)
+    piece = gather_by_exchange(joined, "ep", 0)
     length = piece.shape[0]
     size = length
     while size > 2048 and size % 2 == 0:

time: 137 us -> 133 us (0.971)
  blocking collectives: 69.1 us -> 41.6 us
  waiting for transfers between devices: 27.7 us -> 43.7 us
  starting transfers between devices: 0.12 us -> 5.81 us
  other arithmetic: 4.93 us -> 6.5 us
    all_gather x1 -> x0, blocking collectives: 31.6 us -> none  [local(): piece = lax.all_gather(joined, 'ep', axis=0, tiled=True)]
    all_to_all x0 -> x1, waiting for transfers between devices: none -> 13.2 us  [gather_by_exchange(): return lax.all_to_all(copies, axis, dim, dim, tiled=True)]
    all_to_all x0 -> x1, starting transfers between devices: none -> 5.51 us  [gather_by_exchange(): return lax.all_to_all(copies, axis, dim, dim, tiled=True)]
    all_to_all x1, blocking collectives: 15.8 us -> 19.9 us  [local(): back = lax.all_to_all(home, 'ep', split_axis=0, concat_axis=0, tiled=True)]
    reduce_scatter x1, waiting for transfers between devices: 0.02 us -> 3.73 us  [local(): lax.psum_scatter(worked.astype(jnp.bfloat16), 'tp', scatter_dimension=0,...]
  transfers between devices with their start and end apart: 3 -> 4, of which waited for: 2 -> 4; matrix products, arithmetic and copies ran while one was open for 7% -> 9% of each run, Pallas kernels for 0% -> 0%
where the time goes in v1:
time: 133 us; the launch traced here: 132 us
  waiting for transfers between devices  43.7 us (33%)
  blocking collectives  41.6 us (31%)
  matrix products  17.7 us (13%)
  between operations  14.1 us (11%)
  other arithmetic  6.5 us (5%)
  starting transfers between devices  5.81 us (4%)
  local copies, waits for them, and re-layouts  3.05 us (2%)
    all_to_all x1, blocking collectives, local(): lax.all_to_all(outgoing, 'ep', split_axis=0, concat_axis=0, tiled=True)  21.7 us
    all_to_all x1, blocking collectives, local(): back = lax.all_to_all(home, 'ep', split_axis=0, concat_axis=0, tiled=True)  19.9 us
    all_gather x1, waiting for transfers between devices, local(): piece = lax.all_gather(slot_rows, 'tp', axis=0, tiled=True)  19.6 us
    all_to_all x1, waiting for transfers between devices, gather_by_exchange(): return lax.all_to_all(copies, axis, dim, dim, tiled=True)  13.2 us
    reduce_scatter x1, waiting for transfers between devices, local(): lax.psum_scatter(head_partial.astype(jnp.bfloat16), 'tp', scatter_dimensi...  7.13 us
    all_to_all x1, starting transfers between devices, gather_by_exchange(): return lax.all_to_all(copies, axis, dim, dim, tiled=True)  5.51 us
    dot_general x1, matrix products, local(): gate = jnp.dot(piece, gate_local, preferred_element_type=jnp.float32)  5.14 us
    reduce_scatter x1, waiting for transfers between devices, local(): lax.psum_scatter(worked.astype(jnp.bfloat16), 'tp', scatter_dimension=0,...  3.73 us
  transfers between devices with their start and end apart: 4, of which 4 were waited for; matrix products, arithmetic and copies ran while one was open for 9% of the time, Pallas kernels for 0%

profile of v1, /device:TPU:0, one launch (start us, length us, event | category | flops | bytes accessed | tf_op | source)
XLA Modules:
  0.0 132.4 jit_solution(8977682408791138012)
XLA Ops:
  7.2 0.8 copy.94
  8.7 0.7 multiply_add_fusion
  9.5 1.0 fusion.30
  10.5 1.3 convolution_convert_fusion.1
  11.8 21.7 %all_to_all.22 = bf16[8,16,2048]{2,1,0:T(8,128)(2,1)} all-to-all(bf16[8,16,2048]{2,1,0:T(8,128)(2,1)S(1)} %bitcast.105), channel_id=1, replica_groups=mesh['ep'=8,'tp'=4] {'ep'}, dimensions={0} | all-to-all | bytes 1048576 | tf_op jit(solution)/shard_map/all_to_all | solution.py:133
  33.6 0.8 fusion.37
  34.4 0.8 fusion.38
  35.7 19.6 %all-gather.2.cloned.1.call-done = bf16[512,2048]{1,0:T(8,128)(2,1)} async-done(((bf16[128,2048]{1,0:T(8,128)(2,1)}), bf16[512,2048]{1,0:T(8,128)(2,1)}) %all-gather.2.cloned.1.call-update) | async-done | bytes 2097168 | tf_op jit(solution)/shard_map/all_gather | solution.py:137
  55.3 5.1 %fusion.10 = f32[512,896]{1,0:T(8,128)S(1)} fusion(bf16[512,2048]{1,0:T(8,128)(2,1)} %all-gather.2.cloned.1.call-done, bf16[1,2048,896]{2,1,0:T(8,128)(2,1)} %param.23), kind=kOutput, calls=%fused_computation.11 | convolution fusion | flops 1879048192 | bytes 7602176 | tf_op jit(solution)/shard_map/dot_general | solution.py:138
  60.5 2.4 %multiply_convert_fusion = bf16[512,896]{1,0:T(8,128)(2,1)S(1)} fusion(f32[512,896]{1,0:T(8,128)S(1)} %fusion.10, bf16[512,2048]{1,0:T(8,128)(2,1)S(1)} %copy-done.7, bf16[1,2048,896]{2,1,0:T(8,128)(2,1)S(1)} %copy-done.5), kind=kOutput, calls=%fused_computation.17 | convolution fusion | flops 1881800704 | bytes 8519680 | tf_op jit(solution)/shard_map/dot_general | solution.py:139
  62.9 3.7 %fusion.12 = bf16[32,16,2048]{2,1,0:T(8,128)(2,1)} fusion(bf16[32,16,896]{2,1,0:T(8,128)(2,1)S(1)} %bitcast.108, bf16[1,896,2048]{2,1,0:T(8,128)(2,1)S(1)} %copy-done.6), kind=kOutput, calls=%fused_computation.13 | convolution fusion | flops 1880096768 | bytes 6684672 | tf_op jit(solution)/shard_map/dot_general | solution.py:141
  66.8 0.3 copy.89
  67.1 1.0 copy.90
  68.1 5.5 %all-to-all-start = ((bf16[8,256,128]{1,2,0:T(8,128)(2,1)}), bf16[8,256,128]{1,2,0:T(8,128)(2,1)S(1)}, u32[]{:S(2)}, u32[]{:S(2)}) async-start(bf16[8,256,128]{1,2,0:T(8,128)(2,1)} %copy.90), calls=%async_computation | async-start | bytes 1048576 | tf_op jit(solution)/shard_map/all_to_all | solution.py:13
  74.6 0.3 subtract_convert_fusion
  75.3 13.2 %all-to-all-done = bf16[8,256,128]{1,2,0:T(8,128)(2,1)S(1)} async-done(((bf16[8,256,128]{1,2,0:T(8,128)(2,1)}), bf16[8,256,128]{1,2,0:T(8,128)(2,1)S(1)}, u32[]{:S(2)}, u32[]{:S(2)}) %all-to-all-start) | async-done | bytes 524320 | tf_op jit(solution)/shard_map/all_to_all | solution.py:13
  88.5 1.3 bitcast_reduce_fusion
  89.8 1.4 %fusion.1 = f32[256,4]{0,1:T(4,128)S(1)} fusion(f32[2048,256,4]{1,0,2:T(8,128)S(1)} %get-tuple-element.37, f32[256,4]{0,1:T(4,128)S(1)} %broadcast_maximum_fusion), kind=kLoop, calls=%fused_computation.3 | loop fusion | flops 6290432 | bytes 8396800 | tf_op jit(solution)/shard_map/while/body/eval_jaxpr/reduce_sum | solution.py:80
  91.2 1.5 %fusion.27 = bf16[1,64,256,4]{2,1,3,0:T(8,128)(2,1)S(1)} fusion(f32[2048,256,4]{1,0,2:T(8,128)S(1)} %get-tuple-element.37, f32[256,4]{0,1:T(4,128)S(1)} %broadcast_maximum_fusion, bf16[2048,128]{0,1:T(8,128)(2,1)S(1)} %bitcast.101, f32[256,4]{0,1:T(4,128)S(1)} %get-tuple-element.29, f32[256,4]{0,1:T(4,128)S(1)} %get-tuple-element.28), kind=kOutput, calls=%fused_computation.22 | convolution fusion | flops 274923520 | bytes 8794112 | tf_op jit(solution)/shard_map/while/body/eval_jaxpr/qkgs,skd->qkgd/dot_general | solution.py:81
  92.8 1.4 %convolution_convert_fusion = bf16[256,2048]{1,0:T(8,128)(2,1)} fusion(bf16[256,256]{0,1:T(8,128)(2,1)S(1)} %bitcast.107, bf16[256,2048]{1,0:T(8,128)(2,1)S(1)} %copy-done), kind=kOutput, calls=%fused_computation.14 | convolution fusion | flops 268959744 | bytes 2228224 | tf_op jit(solution)/shard_map/dot_general | solution.py:144
  94.2 3.7 %reduce-scatter.5.cloned.1.call-done = bf16[8,16,2048]{2,1,0:T(8,128)(2,1)} async-done(((bf16[32,16,2048]{2,1,0:T(8,128)(2,1)}), bf16[8,16,2048]{2,1,0:T(8,128)(2,1)}) %reduce-scatter.5.cloned.1.call-update) | async-done | bytes 524304 | tf_op jit(solution)/shard_map/reduce_scatter | solution.py:149
  98.0 19.9 %all_to_all.23 = bf16[8,16,2048]{2,1,0:T(8,128)(2,1)S(1)} all-to-all(bf16[8,16,2048]{2,1,0:T(8,128)(2,1)} %reduce-scatter.5.cloned.1.call-done), channel_id=1, replica_groups=mesh['ep'=8,'tp'=4] {'ep'}, dimensions={0} | all-to-all | bytes 1048576 | tf_op jit(solution)/shard_map/all_to_all | solution.py:155
  117.8 0.9 fusion.17
  118.8 7.1 %reduce-scatter.3.cloned.1.call-done = bf16[64,2048]{1,0:T(8,128)(2,1)} async-done(((bf16[256,2048]{1,0:T(8,128)(2,1)}), bf16[64,2048]{1,0:T(8,128)(2,1)}) %reduce-scatter.3.cloned.1.call-update) | async-done | bytes 262160 | tf_op jit(solution)/shard_map/reduce_scatter | solution.py:146
  (60 shorter events, 2.7 us)
Async XLA Ops:
  7.2 85.6 %copy-start = (bf16[256,2048]{1,0:T(8,128)(2,1)S(1)}, bf16[256,2048]{1,0:T(8,128)(2,1)}, u32[]{:S(2)}) copy-start(bf16[256,2048]{1,0:T(8,128)(2,1)} %param.18) | copy-start | bytes 3145732
  7.2 48.1 %all-gather.2.cloned.1.call-start = ((), (), s32[]{:S(2)}) async-start(), calls=%async_computation.6 | async-start | bytes 2621440 | tf_op jit(solution)/shard_map/all_gather | solution.py:137
  33.5 64.4 %reduce-scatter.5.cloned.1.call-start = ((), (), s32[]{:S(2)}) async-start(), calls=%async_computation.7 | async-start | bytes 2621440 | tf_op jit(solution)/shard_map/reduce_scatter | solution.py:149
  55.3 5.2 %copy-start.5 = (bf16[1,2048,896]{2,1,0:T(8,128)(2,1)S(1)}, bf16[1,2048,896]{2,1,0:T(8,128)(2,1)}, u32[]{:S(2)}) copy-start(bf16[1,2048,896]{2,1,0:T(8,128)(2,1)} %param.24) | copy-start | bytes 11010052
  55.3 5.2 %copy-start.7 = (bf16[512,2048]{1,0:T(8,128)(2,1)S(1)}, bf16[512,2048]{1,0:T(8,128)(2,1)}, u32[]{:S(2)}) copy-start(bf16[512,2048]{1,0:T(8,128)(2,1)} %all-gather.2.cloned.1.call-done) | copy-start | bytes 6291460
  60.5 2.4 %copy-start.6 = (bf16[1,896,2048]{2,1,0:T(8,128)(2,1)S(1)}, bf16[1,896,2048]{2,1,0:T(8,128)(2,1)}, u32[]{:S(2)}) copy-start(bf16[1,896,2048]{2,1,0:T(8,128)(2,1)} %param.25) | copy-start | bytes 11010052
  62.9 3.7 %copy-start.1 = (bf16[256,64]{0,1:T(8,128)(2,1)S(1)}, bf16[256,64]{0,1:T(8,128)(2,1)}, u32[]{:S(2)}) copy-start(bf16[256,64]{0,1:T(8,128)(2,1)} %param.15) | copy-start | bytes 98308
  66.6 7.2 %copy-start.2 = (bf16[256,256]{1,0:T(8,128)(2,1)S(1)}, bf16[256,256]{1,0:T(8,128)(2,1)}, u32[]{:S(2)}) copy-start(bf16[256,256]{1,0:T(8,128)(2,1)} %param.13) | copy-start | bytes 393220
  66.6 7.5 %copy-start.4 = (f32[64]{0:T(128)S(1)}, f32[64]{0:T(128)}, u32[]{:S(2)}) copy-start(f32[64]{0:T(128)} %param.16) | copy-start | bytes 772
  68.1 20.4 %all-to-all-start = ((bf16[8,256,128]{1,2,0:T(8,128)(2,1)}), bf16[8,256,128]{1,2,0:T(8,128)(2,1)S(1)}, u32[]{:S(2)}, u32[]{:S(2)}) async-start(bf16[8,256,128]{1,2,0:T(8,128)(2,1)} %copy.90), calls=%async_computation | async-start | bytes 1048576 | tf_op jit(solution)/shard_map/all_to_all | solution.py:13
  73.6 52.3 %reduce-scatter.3.cloned.1.call-start = ((), (), s32[]{:S(2)}) async-start(), calls=%async_computation.5 | async-start | bytes 1310720 | tf_op jit(solution)/shard_map/reduce_scatter | solution.py:146
  92.8 25.1 %copy-start.3 = (f32[32,2]{0,1:T(2,128)S(1)}, f32[32,2]{0,1:T(2,128)}, u32[]{:S(2)}) copy-start(f32[32,2]{0,1:T(2,128)} %param.22) | copy-start | bytes 772
Sparse Core Ops, SparseCore 0:
  33.7 21.5 all-gather.1
  66.8 31.1 reduce-scatter.4
  101.1 24.7 reduce-scatter.2
